TPU v7x, 32 devices: a whole 2x2x4 slice. The times are simulated.
32 devices in a mesh: kv: 16 (over z, y, x), tp: 2 (over core).
Axes of the slice: x: 2, y: 2, z: 4, core: 2. Of those that a mesh axis runs over, the one named last changes fastest.
Arguments:
- tokens: bfloat16 [256, 2048], P('kv', 'tp'), may hold values from -20 to 20
- attn_gain: bfloat16 [2048], replicated, may hold values from 0.099609375 to 1.8984375
- query_weight: bfloat16 [2048, 1024], P(None, 'tp'), may hold values from -0.125 to 0.125
- key_weight: bfloat16 [2048, 1024], P(None, 'tp'), may hold values from -0.125 to 0.125
- value_weight: bfloat16 [2048, 1024], P(None, 'tp'), may hold values from -0.125 to 0.125
- outgate_weight: bfloat16 [2048, 1024], P(None, 'tp'), may hold values from -0.125 to 0.125
- gate_weight: bfloat16 [2, 8, 2048], replicated, may hold values from -0.125 to 0.125
- forget_bias: float32 [8], replicated, may hold values from -1 to 4
- state_matrix: float32 [256, 8, 128, 128], P('kv', 'tp'), may hold values from -1.8 to 1.8
- state_norm: float32 [256, 8, 128], P('kv', 'tp'), may hold values from -1.8 to 1.8
- state_max: float32 [256, 8], P('kv', 'tp'), may hold values from -1 to 1
- out_weight: bfloat16 [1024, 2048], P(None, 'tp'), may hold values from -0.1875 to 0.1875
- mlp_gain: bfloat16 [2048], P('tp'), may hold values from 0.099609375 to 1.8984375
- up_weight: bfloat16 [2048, 8192], P('tp', 'kv'), may hold values from -0.125 to 0.125
- down_weight: bfloat16 [8192, 2048], P('kv', 'tp'), may hold values from -0.0625 to 0.0625
Outputs:
- result: bfloat16 [256, 2048], P('kv', 'tp')
- next_matrix: float32 [256, 8, 128, 128], P('kv', 'tp')
- next_norm: float32 [256, 8, 128], P('kv', 'tp')
- next_max: float32 [256, 8], P('kv', 'tp')
All inputs are finite; a program needn't handle non-finite values.
Results may differ from a plain program's by a relative error of at most 0.013.
Values may be sent and summed in bfloat16 or wider, within the bound.
A program may use at most 64 MiB of HBM per device.

v0:
```python
import jax
import jax.numpy as jnp
from jax import lax
from jax.sharding import PartitionSpec as P

epsilon = 1e-06


def body(
    tokens,
    attn_gain,
    query_weight,
    key_weight,
    value_weight,
    outgate_weight,
    gate_weight,
    forget_bias,
    state_matrix,
    state_norm,
    state_max,
    out_weight,
    mlp_gain,
    up_weight,
    down_weight,
):
    sequences = tokens.shape[0]
    local_heads = state_matrix.shape[1]
    head_dim = state_matrix.shape[2]
    width = query_weight.shape[1]
    model_width = attn_gain.shape[0]
    first_head = lax.axis_index("tp") * local_heads
    my_gates = lax.dynamic_slice_in_dim(gate_weight, first_head, local_heads, 1).reshape(
        2 * local_heads, model_width
    )
    my_bias = lax.dynamic_slice_in_dim(forget_bias, first_head, local_heads, 0)
    gain_full = attn_gain.astype(jnp.float32)
    seg_values = lax.all_gather(tokens, "tp", axis=1, tiled=True).astype(jnp.float32)
    scaled = (seg_values * gain_full).astype(jnp.bfloat16)

    def product(weight):
        return jnp.dot(scaled, weight, preferred_element_type=jnp.float32)

    gate_part = jnp.einsum("sd,gd->sg", scaled, my_gates, preferred_element_type=jnp.float32)
    squares = jnp.sum(seg_values * seg_values, axis=1)
    query_acc = product(query_weight)
    key_acc = product(key_weight)
    value_acc = product(value_weight)
    outgate_acc = product(outgate_weight)
    scale_in = lax.rsqrt(squares / model_width + epsilon)[:, None]
    query_rows = (query_acc * scale_in).reshape(sequences, local_heads, head_dim)
    key_rows = (key_acc * scale_in * head_dim ** (-0.5)).reshape(sequences, local_heads, head_dim)
    value_rows = (value_acc * scale_in).reshape(sequences, local_heads, head_dim)
    outgate = (outgate_acc * scale_in).reshape(sequences, local_heads, head_dim)
    gate_pre = gate_part * scale_in
    in_gate = gate_pre[:, :local_heads]
    forget_log = jax.nn.log_sigmoid(gate_pre[:, local_heads:] + my_bias)
    next_max = jnp.maximum(forget_log + state_max, in_gate)
    kept_share = jnp.exp(forget_log + state_max - next_max)
    admitted = jnp.exp(in_gate - next_max)
    next_matrix = (
        kept_share[:, :, None, None] * state_matrix
        + admitted[:, :, None, None] * key_rows[:, :, :, None] * value_rows[:, :, None, :]
    )
    next_norm = kept_share[:, :, None] * state_norm + admitted[:, :, None] * key_rows
    numerator = jnp.einsum(
        "shd,shde->she", query_rows, next_matrix, precision=lax.Precision.HIGHEST
    )
    denominator = jnp.sum(query_rows * next_norm, axis=2)
    head_out = numerator / jnp.maximum(jnp.abs(denominator), 1.0)[:, :, None]
    mixed = (head_out * jax.nn.sigmoid(outgate)).reshape(sequences, width).astype(jnp.bfloat16)
    attended = jnp.dot(
        lax.all_gather(mixed, "tp", axis=1, tiled=True),
        out_weight,
        preferred_element_type=jnp.float32,
    )
    residual = (tokens.astype(jnp.float32) + attended).astype(jnp.bfloat16)
    gain_mid = mlp_gain.astype(jnp.float32)
    rows_all = lax.all_gather(residual, "kv", axis=0, tiled=True)
    row_values = rows_all.astype(jnp.float32)
    row_squares = jnp.sum(row_values * row_values, axis=1)
    scaled_mid = (row_values * gain_mid).astype(jnp.bfloat16)
    partial_value = jnp.dot(scaled_mid, up_weight, preferred_element_type=jnp.float32)
    summed = lax.psum(partial_value.astype(jnp.bfloat16), "tp").astype(jnp.float32)
    total_squares = lax.psum(row_squares.astype(jnp.bfloat16), "tp").astype(jnp.float32)
    up_value = summed * lax.rsqrt(total_squares / model_width + epsilon)[:, None]
    hidden = jnp.square(jax.nn.relu(up_value)).astype(jnp.bfloat16)
    mixer_out = lax.psum_scatter(
        jnp.dot(hidden, down_weight, preferred_element_type=jnp.float32),
        "kv",
        scatter_dimension=0,
        tiled=True,
    )
    result = (residual.astype(jnp.float32) + mixer_out).astype(jnp.bfloat16)
    return (result, next_matrix, next_norm, next_max)


def solution(mesh):
    in_specs = (
        P("kv", "tp"),
        P(),
        P(None, "tp"),
        P(None, "tp"),
        P(None, "tp"),
        P(None, "tp"),
        P(),
        P(),
        P("kv", "tp", None, None),
        P("kv", "tp", None),
        P("kv", "tp"),
        P(None, "tp"),
        P("tp"),
        P("tp", "kv"),
        P("kv", "tp"),
    )
    out_specs = (P("kv", "tp"), P("kv", "tp", None, None), P("kv", "tp", None), P("kv", "tp"))
    return jax.shard_map(body, mesh=mesh, in_specs=in_specs, out_specs=out_specs, check_vma=False)
```

profile of v0, /device:TPU:0, one launch (start us, length us, event | category | flops | bytes accessed | tf_op | source)
XLA Modules:
  0.0 179.5 jit_solution(18217517377536054853)
XLA Ops:
  7.3 0.8 convert_element_type.53
  8.1 2.2 %all_gather.9 = bf16[16,2048]{1,0:T(8,128)(2,1)S(1)} all-gather(bf16[16,1024]{1,0:T(8,128)(2,1)} %param.15), channel_id=1, replica_groups=mesh['kv'=16,'tp'=2] {'tp'}, dimensions={1}, use_global_device_ids=true | all-gather | bytes 98304 | tf_op jit(solution)/shard_map/all_gather | solution.py:37
  10.3 0.1 fusion.14
  10.4 1.9 %convolution_multiply_fusion.3 = f32[16,512]{1,0:T(8,128)S(1)} fusion(bf16[2048,512]{1,0:T(8,128)(2,1)} %param.17, bf16[16,2048]{1,0:T(8,128)(2,1)S(1)} %all_gather.9, f32[2048]{0:T(1024)S(1)} %convert_element_type.53, f32[16]{0:T(128)S(1)} %add_rsqrt_fusion.1), kind=kOutput, calls=%fused_computation.11 | convolution fusion | flops 33660928 | bytes 2203712 | tf_op jit(solution)/shard_map/dot_general | solution.py:41
  12.6 0.1 convolution_multiply_fusion.4
  12.8 0.1 subtract_exponential_fusion.1
  12.9 0.1 copy.19
  13.1 1.9 %fusion.3 = f32[16,512]{1,0:T(8,128)S(1)} fusion(bf16[2048,512]{1,0:T(8,128)(2,1)} %param.18, bf16[16,2048]{1,0:T(8,128)(2,1)S(1)} %all_gather.9, f32[2048]{0:T(1024)S(1)} %convert_element_type.53, f32[16]{0:T(128)S(1)} %add_rsqrt_fusion.1), kind=kOutput, calls=%fused_computation.12 | convolution fusion | flops 33669120 | bytes 2203712 | tf_op jit(solution)/shard_map/dot_general | solution.py:41
  15.1 0.7 multiply_reduce_fusion
  15.8 1.9 %convolution_multiply_fusion.1 = f32[16,512]{1,0:T(8,128)S(1)} fusion(bf16[2048,512]{1,0:T(8,128)(2,1)} %param.19, bf16[16,2048]{1,0:T(8,128)(2,1)S(1)} %all_gather.9, f32[2048]{0:T(1024)S(1)} %convert_element_type.53, f32[16]{0:T(128)S(1)} %add_rsqrt_fusion.1), kind=kOutput, calls=%fused_computation.9 | convolution fusion | flops 33660928 | bytes 2203712 | tf_op jit(solution)/shard_map/dot_general | solution.py:41
  17.8 0.4 fusion.5
  18.2 3.0 %multiply_add_fusion = f32[16,4,128,128]{3,2,1,0:T(8,128)S(1)} fusion(f32[16,4,128,128]{3,2,1,0:T(8,128)} %param.23, f32[16,4,128]{2,1,0:T(4,128)S(1)} %mul.144, f32[16,4,128]{2,1,0:T(4,128)S(1)} %get-tuple-element.6, f32[16,4]{1,0:T(8,128)S(1)} %copy.19), kind=kLoop, calls=%fused_computation | loop fusion | flops 3145728 | bytes 8454400 | tf_op jit(solution)/shard_map/add | solution.py:61
  21.3 3.7 %fusion.24 = f32[16,4,1,128]{3,2,1,0:T(1,128)S(1)} fusion(f32[16,4,128,1]{2,3,1,0:T(1,128)S(1)} %bitcast.18, f32[16,4,128,128]{3,2,1,0:T(8,128)S(1)} %multiply_add_fusion), kind=kOutput, calls=%fused_computation.45 | convolution fusion | flops 12582912 | bytes 4259840 | tf_op jit(solution)/shard_map/shd,shde->she/dot_general | solution.py:65
  25.0 0.1 fusion.15
  25.1 2.0 %all_gather.10 = bf16[16,1024]{1,0:T(8,128)(2,1)S(1)} all-gather(bf16[16,512]{1,0:T(8,128)(2,1)S(1)} %bitcast.20), channel_id=1, replica_groups=mesh['kv'=16,'tp'=2] {'tp'}, dimensions={1}, use_global_device_ids=true | all-gather | bytes 49152 | tf_op jit(solution)/shard_map/all_gather | solution.py:72
  27.0 0.4 fusion
  27.4 45.4 %all_gather.11 = bf16[256,1024]{1,0:T(8,128)(2,1)S(1)} all-gather(bf16[16,1024]{1,0:T(8,128)(2,1)S(1)} %fusion), channel_id=1, replica_groups=mesh['kv'=16,'tp'=2] {'kv'}, dimensions={0}, use_global_device_ids=true | all-gather | bytes 557056 | tf_op jit(solution)/shard_map/all_gather | solution.py:78
  72.8 1.2 convolution_convert_fusion
  74.1 0.2 fusion.7
  74.2 2.5 %psum.15 = bf16[256]{0:T(256)(128)(2,1)S(1)} all-reduce(bf16[256]{0:T(256)(128)(2,1)S(1)} %fusion.7), channel_id=1, replica_groups=mesh['kv'=16,'tp'=2] {'tp'}, use_global_device_ids=true, to_apply=%region_4.5 | all-reduce | flops 256 | bytes 1024 | tf_op jit(solution)/shard_map/psum | solution.py:84
  76.7 11.5 %all-reduce.2.cloned.1.call-done = bf16[256,512]{1,0:T(8,128)(2,1)} async-done(((bf16[256,512]{1,0:T(8,128)(2,1)}), bf16[256,512]{1,0:T(8,128)(2,1)}) %all-reduce.2.cloned.1.call-update) | async-done | bytes 262160 | tf_op jit(solution)/shard_map/psum | solution.py:83
  88.3 2.8 %fusion.10 = f32[256,1024]{1,0:T(8,128)} fusion(bf16[512,1024]{1,0:T(8,128)(2,1)} %param.29, bf16[256,512]{1,0:T(8,128)(2,1)} %all-reduce.2.cloned.1.call-done, f32[256]{0:T(256)S(1)} %add_rsqrt_fusion), kind=kOutput, calls=%fused_computation.20 | convolution fusion | flops 269090816 | bytes 2360320 | tf_op jit(solution)/shard_map/dot_general | solution.py:88
  91.1 80.1 %reduce-scatter.2.cloned.1.call-done = f32[16,1024]{1,0:T(8,128)} async-done(((f32[256,1024]{1,0:T(8,128)}), f32[16,1024]{1,0:T(8,128)}) %reduce-scatter.2.cloned.1.call-update) | async-done | bytes 65552 | tf_op jit(solution)/shard_map/reduce_scatter | solution.py:87
  171.2 1.5 add_convert_fusion
  (41 shorter events, 0.6 us)
Async XLA Ops:
  7.2 19.9 %copy-start = (bf16[1024,1024]{1,0:T(8,128)(2,1)S(1)}, bf16[1024,1024]{1,0:T(8,128)(2,1)}, u32[]{:S(2)}) copy-start(bf16[1024,1024]{1,0:T(8,128)(2,1)} %param.26) | copy-start | bytes 6291460
  7.2 5.3 %copy-start.7 = (bf16[1024]{0:T(1024)(128)(2,1)S(1)}, bf16[1024]{0:T(1024)(128)(2,1)}, u32[]{:S(2)}) copy-start(bf16[1024]{0:T(1024)(128)(2,1)} %param.27) | copy-start | bytes 6148
  7.2 5.3 %copy-start.10 = (f32[8]{0:T(128)S(1)}, f32[8]{0:T(128)}, u32[]{:S(2)}) copy-start(f32[8]{0:T(128)} %param.22) | copy-start | bytes 100
  7.2 5.4 %copy-start.5 = (bf16[2,8,2048]{2,1,0:T(8,128)(2,1)S(1)}, bf16[2,8,2048]{2,1,0:T(8,128)(2,1)}, u32[]{:S(2)}) copy-start(bf16[2,8,2048]{2,1,0:T(8,128)(2,1)} %param.21) | copy-start | bytes 196612
  7.2 5.6 %copy-start.8 = (f32[16,4]{0,1:T(4,128)S(1)}, f32[16,4]{0,1:T(4,128)}, u32[]{:S(2)}) copy-start(f32[16,4]{0,1:T(4,128)} %param.25) | copy-start | bytes 772
  7.2 81.0 %all-reduce.2.cloned.1.call-start = ((), (), s32[]{:S(2)}) async-start(), calls=%async_computation.1 | async-start | bytes 524288 | tf_op jit(solution)/shard_map/psum | solution.py:83
  10.4 4.6 %copy-start.4 = (f32[16,4,128]{2,1,0:T(4,128)S(1)}, f32[16,4,128]{2,1,0:T(4,128)}, u32[]{:S(2)}) copy-start(f32[16,4,128]{2,1,0:T(4,128)} %param.24) | copy-start | bytes 98308
  12.9 4.9 %copy-start.6 = (f32[16,4]{0,1:T(4,128)}, f32[16,4]{0,1:T(4,128)S(1)}, u32[]{:S(2)}) copy-start(f32[16,4]{0,1:T(4,128)S(1)} %get-tuple-element.8) | copy-start | bytes 772
  15.1 2.7 %copy-start.2 = (bf16[2048,512]{1,0:T(8,128)(2,1)S(1)}, bf16[2048,512]{1,0:T(8,128)(2,1)}, u32[]{:S(2)}) copy-start(bf16[2048,512]{1,0:T(8,128)(2,1)} %param.20) | copy-start | bytes 6291460
  21.3 3.7 %copy-start.1 = (f32[16,4,128,128]{3,2,1,0:T(8,128)}, f32[16,4,128,128]{3,2,1,0:T(8,128)S(1)}, u32[]{:S(2)}) copy-start(f32[16,4,128,128]{3,2,1,0:T(8,128)S(1)} %multiply_add_fusion) | copy-start | bytes 12582916
  21.3 5.8 %copy-start.3 = (bf16[16,1024]{1,0:T(8,128)(2,1)S(1)}, bf16[16,1024]{1,0:T(8,128)(2,1)}, u32[]{:S(2)}) copy-start(bf16[16,1024]{1,0:T(8,128)(2,1)} %param.15) | copy-start | bytes 98308
  25.0 47.9 %copy-start.9 = (bf16[1024,512]{1,0:T(8,128)(2,1)S(1)}, bf16[1024,512]{1,0:T(8,128)(2,1)}, u32[]{:S(2)}) copy-start(bf16[1024,512]{1,0:T(8,128)(2,1)} %param.28) | copy-start | bytes 3145732
  74.0 97.2 %reduce-scatter.2.cloned.1.call-start = ((), (), s32[]{:S(2)}) async-start(), calls=%async_computation.2 | async-start | bytes 1114112 | tf_op jit(solution)/shard_map/reduce_scatter | solution.py:87
Sparse Core Ops, SparseCore 0:
  74.1 14.0 all-reduce.1
  91.2 79.9 reduce-scatter.1
where the time goes:
time: 180 us; the launch traced here: 179 us
  waiting for transfers between devices  91.7 us (51%)
  blocking collectives  52 us (29%)
  matrix products  14.3 us (8%)
  between operations  14.3 us (8%)
  other arithmetic  6.56 us (4%)
    reduce_scatter x1, waiting for transfers between devices, body(): lax.psum_scatter(jnp.dot(hidden, down_weight, preferred_element_type=jnp....  80.1 us
    all_gather x1, blocking collectives, body(): rows_all = lax.all_gather(residual, 'kv', axis=0, tiled=True)  45.4 us
    psum x1, waiting for transfers between devices, body(): lax.psum(partial_value.astype(jnp.bfloat16), 'tp').astype(jnp.float32)  11.5 us
    dot_general x4, matrix products, product(): return jnp.dot(scaled, weight, preferred_element_type=jnp.float32)  6.2 us
    dot_general x1, matrix products, body(): jnp.einsum('shd,shde->she', query_rows, next_matrix, precision=lax.Precis...  3.66 us
  transfers between devices with their start and end apart: 2, of which 2 were waited for; matrix products, arithmetic and copies ran while one was open for 0% of the time, Pallas kernels for 0%

commit v1 on v0

--- a/solution.py
+++ b/solution.py
@@ -80,7 +80,9 @@
     row_squares = jnp.sum(row_values * row_values, axis=1)
     scaled_mid = (row_values * gain_mid).astype(jnp.bfloat16)
     partial_value = jnp.dot(scaled_mid, up_weight, preferred_element_type=jnp.float32)
-    summed = lax.psum(partial_value.astype(jnp.bfloat16), "tp").astype(jnp.float32)
+    summed = jnp.sum(lax.all_gather(partial_value.astype(jnp.bfloat16), "tp"), axis=0).astype(
+        jnp.float32
+    )
     total_squares = lax.psum(row_squares.astype(jnp.bfloat16), "tp").astype(jnp.float32)
     up_value = summed * lax.rsqrt(total_squares / model_width + epsilon)[:, None]
     hidden = jnp.square(jax.nn.relu(up_value)).astype(jnp.bfloat16)

time: 180 us -> 165 us (0.917)
  waiting for transfers between devices: 91.7 us -> 74.7 us
  blocking collectives: 52 us -> 54.1 us
    psum x1 -> x0, waiting for transfers between devices: 11.5 us -> none  [body(): lax.psum(partial_value.astype(jnp.bfloat16), 'tp').astype(jnp.float32)]
    reduce_scatter x1, waiting for transfers between devices: 80.1 us -> 74.7 us  [body(): lax.psum_scatter(jnp.dot(hidden, down_weight, preferred_element_type=jnp....]
    all_gather x0 -> x1, blocking collectives: none -> 2.18 us  [body(): lax.all_gather(partial_value.astype(jnp.bfloat16), 'tp')]
  transfers between devices with their start and end apart: 2 -> 1, of which waited for: 2 -> 1; matrix products, arithmetic and copies ran while one was open for 0% -> 0% of each run, Pallas kernels for 0% -> 0%
where the time goes in v1:
time: 165 us
  waiting for transfers between devices  74.7 us (45%)
  blocking collectives  54.1 us (33%)
  matrix products  14.8 us (9%)
  between operations  14.3 us (9%)
  other arithmetic  6.65 us (4%)
    reduce_scatter x1, waiting for transfers between devices, body(): lax.psum_scatter(jnp.dot(hidden, down_weight, preferred_element_type=jnp....  74.7 us
    all_gather x1, blocking collectives, body(): rows_all = lax.all_gather(residual, 'kv', axis=0, tiled=True)  45.4 us
    dot_general x4, matrix products, product(): return jnp.dot(scaled, weight, preferred_element_type=jnp.float32)  6.2 us
    dot_general x1, matrix products, body(): jnp.einsum('shd,shde->she', query_rows, next_matrix, precision=lax.Precis...  3.66 us
  transfers between devices with their start and end apart: 1, of which 1 were waited for; matrix products, arithmetic and copies ran while one was open for 0% of the time, Pallas kernels for 0%

profile of v1, /device:TPU:0, one launch (start us, length us, event | category | flops | bytes accessed | tf_op | source)
XLA Modules:
  0.0 165.1 jit_solution(2728732152902404376)
XLA Ops:
  7.3 0.8 convert_element_type.55
  8.1 2.2 %all_gather.15 = bf16[16,2048]{1,0:T(8,128)(2,1)S(1)} all-gather(bf16[16,1024]{1,0:T(8,128)(2,1)} %param.15), channel_id=1, replica_groups=mesh['kv'=16,'tp'=2] {'tp'}, dimensions={1}, use_global_device_ids=true | all-gather | bytes 98304 | tf_op jit(solution)/shard_map/all_gather | solution.py:37
  10.3 0.1 fusion.14
  10.4 1.9 %convolution_multiply_fusion.3 = f32[16,512]{1,0:T(8,128)S(1)} fusion(bf16[2048,512]{1,0:T(8,128)(2,1)} %param.17, bf16[16,2048]{1,0:T(8,128)(2,1)S(1)} %all_gather.15, f32[2048]{0:T(1024)S(1)} %convert_element_type.55, f32[16]{0:T(128)S(1)} %add_rsqrt_fusion.1), kind=kOutput, calls=%fused_computation.11 | convolution fusion | flops 33660928 | bytes 2203712 | tf_op jit(solution)/shard_map/dot_general | solution.py:41
  12.6 0.1 convolution_multiply_fusion.4
  12.8 0.1 subtract_exponential_fusion.1
  13.1 1.9 %fusion.3 = f32[16,512]{1,0:T(8,128)S(1)} fusion(bf16[2048,512]{1,0:T(8,128)(2,1)} %param.18, bf16[16,2048]{1,0:T(8,128)(2,1)S(1)} %all_gather.15, f32[2048]{0:T(1024)S(1)} %convert_element_type.55, f32[16]{0:T(128)S(1)} %add_rsqrt_fusion.1), kind=kOutput, calls=%fused_computation.12 | convolution fusion | flops 33669120 | bytes 2203712 | tf_op jit(solution)/shard_map/dot_general | solution.py:41
  15.1 0.7 multiply_reduce_fusion
  15.8 1.9 %convolution_multiply_fusion.1 = f32[16,512]{1,0:T(8,128)S(1)} fusion(bf16[2048,512]{1,0:T(8,128)(2,1)} %param.19, bf16[16,2048]{1,0:T(8,128)(2,1)S(1)} %all_gather.15, f32[2048]{0:T(1024)S(1)} %convert_element_type.55, f32[16]{0:T(128)S(1)} %add_rsqrt_fusion.1), kind=kOutput, calls=%fused_computation.9 | convolution fusion | flops 33660928 | bytes 2203712 | tf_op jit(solution)/shard_map/dot_general | solution.py:41
  17.8 0.4 fusion.5
  18.2 3.0 %multiply_add_fusion = f32[16,4,128,128]{3,2,1,0:T(8,128)S(1)} fusion(f32[16,4,128,128]{3,2,1,0:T(8,128)} %param.23, f32[16,4,128]{2,1,0:T(4,128)S(1)} %mul.144, f32[16,4,128]{2,1,0:T(4,128)S(1)} %get-tuple-element.6, f32[16,4]{1,0:T(8,128)S(1)} %copy.19), kind=kLoop, calls=%fused_computation | loop fusion | flops 3145728 | bytes 8454400 | tf_op jit(solution)/shard_map/add | solution.py:61
  21.3 3.7 %fusion.24 = f32[16,4,1,128]{3,2,1,0:T(1,128)S(1)} fusion(f32[16,4,128,1]{2,3,1,0:T(1,128)S(1)} %bitcast.20, f32[16,4,128,128]{3,2,1,0:T(8,128)S(1)} %multiply_add_fusion), kind=kOutput, calls=%fused_computation.45 | convolution fusion | flops 12582912 | bytes 4259840 | tf_op jit(solution)/shard_map/shd,shde->she/dot_general | solution.py:65
  25.0 0.1 fusion.15
  25.1 1.8 %all_gather.16 = bf16[16,1024]{1,0:T(8,128)(2,1)S(1)} all-gather(bf16[16,512]{1,0:T(8,128)(2,1)S(1)} %bitcast.22), channel_id=1, replica_groups=mesh['kv'=16,'tp'=2] {'tp'}, dimensions={1}, use_global_device_ids=true | all-gather | bytes 49152 | tf_op jit(solution)/shard_map/all_gather | solution.py:72
  26.9 0.4 fusion
  27.3 45.4 %all_gather.17 = bf16[256,1024]{1,0:T(8,128)(2,1)S(1)} all-gather(bf16[16,1024]{1,0:T(8,128)(2,1)S(1)} %fusion), channel_id=1, replica_groups=mesh['kv'=16,'tp'=2] {'kv'}, dimensions={0}, use_global_device_ids=true | all-gather | bytes 557056 | tf_op jit(solution)/shard_map/all_gather | solution.py:78
  72.7 0.2 fusion.7
  72.9 2.5 %psum.7 = bf16[256]{0:T(256)(128)(2,1)S(1)} all-reduce(bf16[256]{0:T(256)(128)(2,1)S(1)} %fusion.7), channel_id=1, replica_groups=mesh['kv'=16,'tp'=2] {'tp'}, use_global_device_ids=true, to_apply=%region_4.5 | all-reduce | flops 256 | bytes 1024 | tf_op jit(solution)/shard_map/psum | solution.py:86
  75.3 1.7 %convolution_convert_fusion = bf16[256,512]{1,0:T(8,128)(2,1)S(1)} fusion(bf16[1024,512]{1,0:T(8,128)(2,1)} %param.28, bf16[256,1024]{1,0:T(8,128)(2,1)S(1)} %all_gather.17, f32[1024]{0:T(1024)S(1)} %convert_element_type.62), kind=kOutput, calls=%fused_computation.3 | convolution fusion | flops 269352960 | bytes 1839104 | tf_op jit(solution)/shard_map/dot_general | solution.py:82
  77.0 2.2 %all-gather = bf16[512,512]{1,0:T(8,128)(2,1)S(1)} all-gather(bf16[256,512]{1,0:T(8,128)(2,1)S(1)} %convolution_convert_fusion), channel_id=2, replica_groups=mesh['kv'=16,'tp'=2] {'tp'}, dimensions={0}, use_global_device_ids=true | all-gather | bytes 786432 | tf_op jit(solution)/shard_map/all_gather | solution.py:83
  79.2 0.1 reduce_sum.41
  79.3 2.7 %fusion.10 = f32[256,1024]{1,0:T(8,128)} fusion(bf16[512,1024]{1,0:T(8,128)(2,1)} %param.29, bf16[256,512]{1,0:T(8,128)(2,1)S(1)} %reduce_sum.41, f32[256]{0:T(256)S(1)} %add_rsqrt_fusion), kind=kOutput, calls=%fused_computation.20 | convolution fusion | flops 269090816 | bytes 2360320 | tf_op jit(solution)/shard_map/dot_general | solution.py:90
  82.1 74.7 %reduce-scatter.2.cloned.1.call-done = f32[16,1024]{1,0:T(8,128)} async-done(((f32[256,1024]{1,0:T(8,128)}), f32[16,1024]{1,0:T(8,128)}) %reduce-scatter.2.cloned.1.call-update) | async-done | bytes 65552 | tf_op jit(solution)/shard_map/reduce_scatter | solution.py:89
  156.7 1.5 add_convert_fusion
  (38 shorter events, 0.6 us)
Async XLA Ops:
  7.2 19.7 %copy-start = (bf16[1024,1024]{1,0:T(8,128)(2,1)S(1)}, bf16[1024,1024]{1,0:T(8,128)(2,1)}, u32[]{:S(2)}) copy-start(bf16[1024,1024]{1,0:T(8,128)(2,1)} %param.26) | copy-start | bytes 6291460
  7.2 5.3 %copy-start.7 = (bf16[1024]{0:T(1024)(128)(2,1)S(1)}, bf16[1024]{0:T(1024)(128)(2,1)}, u32[]{:S(2)}) copy-start(bf16[1024]{0:T(1024)(128)(2,1)} %param.27) | copy-start | bytes 6148
  7.2 5.3 %copy-start.9 = (f32[8]{0:T(128)S(1)}, f32[8]{0:T(128)}, u32[]{:S(2)}) copy-start(f32[8]{0:T(128)} %param.22) | copy-start | bytes 100
  7.2 5.4 %copy-start.5 = (bf16[2,8,2048]{2,1,0:T(8,128)(2,1)S(1)}, bf16[2,8,2048]{2,1,0:T(8,128)(2,1)}, u32[]{:S(2)}) copy-start(bf16[2,8,2048]{2,1,0:T(8,128)(2,1)} %param.21) | copy-start | bytes 196612
  7.2 5.6 %copy-start.8 = (f32[16,4]{0,1:T(4,128)S(1)}, f32[16,4]{0,1:T(4,128)}, u32[]{:S(2)}) copy-start(f32[16,4]{0,1:T(4,128)} %param.25) | copy-start | bytes 772
  7.2 149.5 %reduce-scatter.2.cloned.1.call-start = ((), (), s32[]{:S(2)}) async-start(), calls=%async_computation.1 | async-start | bytes 1114112 | tf_op jit(solution)/shard_map/reduce_scatter | solution.py:89
  10.4 4.6 %copy-start.4 = (f32[16,4,128]{2,1,0:T(4,128)S(1)}, f32[16,4,128]{2,1,0:T(4,128)}, u32[]{:S(2)}) copy-start(f32[16,4,128]{2,1,0:T(4,128)} %param.24) | copy-start | bytes 98308
  12.9 4.9 %copy-start.6 = (f32[16,4]{0,1:T(4,128)}, f32[16,4]{0,1:T(4,128)S(1)}, u32[]{:S(2)}) copy-start(f32[16,4]{0,1:T(4,128)S(1)} %get-tuple-element.8) | copy-start | bytes 772
  15.1 2.7 %copy-start.2 = (bf16[2048,512]{1,0:T(8,128)(2,1)S(1)}, bf16[2048,512]{1,0:T(8,128)(2,1)}, u32[]{:S(2)}) copy-start(bf16[2048,512]{1,0:T(8,128)(2,1)} %param.20) | copy-start | bytes 6291460
  21.3 3.7 %copy-start.1 = (f32[16,4,128,128]{3,2,1,0:T(8,128)}, f32[16,4,128,128]{3,2,1,0:T(8,128)S(1)}, u32[]{:S(2)}) copy-start(f32[16,4,128,128]{3,2,1,0:T(8,128)S(1)} %multiply_add_fusion) | copy-start | bytes 12582916
  21.3 5.6 %copy-start.3 = (bf16[16,1024]{1,0:T(8,128)(2,1)S(1)}, bf16[16,1024]{1,0:T(8,128)(2,1)}, u32[]{:S(2)}) copy-start(bf16[16,1024]{1,0:T(8,128)(2,1)} %param.15) | copy-start | bytes 98308
Sparse Core Ops, SparseCore 0:
  82.2 74.5 reduce-scatter.1
